TPU v7x, 32 devices: a whole 2x2x4 slice. The times are simulated.
32 devices in a mesh: sp: 8 (over z, core), tp: 4 (over y, x).
Axes of the slice: x: 2, y: 2, z: 4, core: 2. Of those that a mesh axis runs over, the one named last changes fastest.
Arguments:
- wide_queries: bfloat16 [512, 2560], P('sp', 'tp'), may hold values from -512 to 512
- narrow_queries: bfloat16 [512, 1536], P('sp', 'tp'), may hold values from -512 to 512
- kv_latent: bfloat16 [512, 512], P('sp'), may hold values from -6 to 6
- rope_key: bfloat16 [512, 32], P('sp'), may hold values from -4 to 4
- latent_gain: float32 [512], replicated, may hold values from 0.1 to 1.9
- wide_kv_weight: bfloat16 [512, 4096], P(None, 'tp'), may hold values from -0.25 to 0.25
- narrow_kv_weight: bfloat16 [512, 2048], P(None, 'tp'), may hold values from -0.25 to 0.25
- wide_out_weight: bfloat16 [2048, 2048], P('tp'), may hold values from -0.4375 to 0.4375
- narrow_out_weight: bfloat16 [1024, 2048], P('tp'), may hold values from -0.4375 to 0.4375
- residual: bfloat16 [512, 2048], P('sp'), may hold values from -6 to 6
- norm_gain: float32 [2048], replicated, may hold values from 0.1 to 1.9
- route_ids: int32 [512, 2], P('sp'), may hold values from 0 to 15, all different within a row; in each aligned block of 64 rows (0 to 63, 64 to 127, ...) at most 12 rows name the same one
- route_weights: float32 [512, 2], P('sp'), may hold values from 0.3 to 1.3
- expert_gate: bfloat16 [16, 2048, 1024], P('sp', None, 'tp'), may hold values from -0.125 to 0.125
- expert_up: bfloat16 [16, 2048, 1024], P('sp', None, 'tp'), may hold values from -0.125 to 0.125
- expert_down: bfloat16 [16, 1024, 2048], P('sp', 'tp'), may hold values from -0.1875 to 0.1875
- shared_gate: bfloat16 [2048, 1024], P(None, 'tp'), may hold values from -0.125 to 0.125
- shared_up: bfloat16 [2048, 1024], P(None, 'tp'), may hold values from -0.125 to 0.125
- shared_down: bfloat16 [1024, 2048], P('tp'), may hold values from -0.1875 to 0.1875
Outputs:
- mixed_out: bfloat16 [512, 2048], P('sp', 'tp')
Inputs may be any that keep to these rules, and one draw needn't show every extreme that they name: `route_ids`: in the rows of one index of sp (aligned blocks of 64 rows) no expert is named by more than 12 rows, and some expert by exactly that many; each row names 2 different experts.
All inputs are finite; a program needn't handle non-finite values.
Results may differ from a plain program's by a relative error of at most 0.018.
Values may be sent and summed in bfloat16 or wider, within the bound.
A program may use at most 64 MiB of HBM per device.

v0:
```python
import jax
import jax.numpy as jnp
from jax import lax
from jax.sharding import PartitionSpec as P

D_MODEL = 2048
WIDE_NOPE = 128
WIDE_VALUE = 128
NARROW_NOPE = 64
NARROW_VALUE = 64
ROPE_DIM = 32
THETA = 10000.0
EPS = 1e-06
FLOOR = -1e30


def rounded(values):
    return lax.optimization_barrier(values.astype(jnp.bfloat16)).astype(jnp.float32)


def rotate(values, positions):
    half_width = values.shape[-1] // 2
    frequency = THETA ** (-2.0 * jnp.arange(half_width, dtype=jnp.float32) / values.shape[-1])
    angles = positions.astype(jnp.float32)[:, None] * frequency[None, :]
    if values.ndim == 3:
        angles = angles[:, None, :]
    cosine = jnp.cos(angles)
    sine_part = jnp.sin(angles)
    as_float = values.astype(jnp.float32)
    first_half = as_float[..., :half_width]
    second_half = as_float[..., half_width:]
    return jnp.concatenate(
        [
            first_half * cosine - second_half * sine_part,
            second_half * cosine + first_half * sine_part,
        ],
        axis=-1,
    ).astype(jnp.bfloat16)


def rms_scale(values, gain):
    as_float = values.astype(jnp.float32)
    scaled = as_float * lax.rsqrt(jnp.mean(as_float * as_float, axis=-1, keepdims=True) + EPS)
    return (scaled * gain).astype(jnp.bfloat16)


def fresh_state(head_count, query_count, value_width):
    return (
        jnp.full((head_count, query_count), FLOOR, jnp.float32),
        jnp.zeros((head_count, query_count), jnp.float32),
        jnp.zeros((head_count, query_count, value_width), jnp.float32),
    )


def update(carry_part, queries, nope_width, kv_rows, rot_rows, query_pos, key_pos):
    row_peak, row_total, summed = carry_part
    head_count = queries.shape[1]
    key_value = kv_rows.reshape(kv_rows.shape[0], head_count, -1)
    values = key_value[..., nope_width:]
    shared_rot = jnp.broadcast_to(
        rot_rows[:, None, :], (rot_rows.shape[0], head_count, rot_rows.shape[1])
    )
    whole_keys = jnp.concatenate([key_value[..., :nope_width], shared_rot], axis=-1)
    scores = jnp.einsum("qhd,khd->hqk", queries, whole_keys, preferred_element_type=jnp.float32)
    scores = scores * queries.shape[-1] ** (-0.5)
    allowed = (query_pos[:, None] >= key_pos[None, :])[None]
    newest = jnp.maximum(row_peak, jnp.max(jnp.where(allowed, scores, FLOOR), axis=-1))
    weights = jnp.where(allowed, jnp.exp(scores - newest[..., None]), 0.0)
    row_total = jnp.sum(weights, axis=-1)
    summed = jnp.einsum(
        "hqk,khv->hqv", weights.astype(jnp.bfloat16), values, preferred_element_type=jnp.float32
    )
    return (newest, row_total, summed)


def local(
    wide_queries,
    narrow_queries,
    kv_latent,
    rope_key,
    latent_gain,
    wide_kv_weight,
    narrow_kv_weight,
    wide_out_weight,
    narrow_out_weight,
    residual,
    norm_gain,
    route_ids,
    route_weights,
    expert_gate,
    expert_up,
    expert_down,
    shared_gate,
    shared_up,
    shared_down,
):
    tok_rows = residual.shape[0]
    positions = lax.axis_index("sp") * tok_rows + jnp.arange(tok_rows, dtype=jnp.int32)
    wide_count = wide_out_weight.shape[0] // WIDE_VALUE
    narrow_count = narrow_out_weight.shape[0] // NARROW_VALUE
    wide_q = wide_queries.reshape(tok_rows, wide_count, WIDE_NOPE + ROPE_DIM)
    wide_q = jnp.concatenate(
        [wide_q[..., :WIDE_NOPE], rotate(wide_q[..., WIDE_NOPE:], positions)], axis=-1
    )
    narrow_q = narrow_queries.reshape(tok_rows, narrow_count, NARROW_NOPE + ROPE_DIM)
    narrow_q = jnp.concatenate(
        [narrow_q[..., :NARROW_NOPE], rotate(narrow_q[..., NARROW_NOPE:], positions)], axis=-1
    )
    key_rot = rotate(rope_key, positions)
    latent = rms_scale(kv_latent, latent_gain)
    initial = (
        fresh_state(wide_count, tok_rows, WIDE_VALUE),
        fresh_state(narrow_count, tok_rows, NARROW_VALUE),
    )
    pieces = (
        lax.all_gather(latent, "sp", axis=0, tiled=True),
        lax.all_gather(key_rot, "sp", axis=0, tiled=True),
    )
    wide_rows = jnp.dot(pieces[0], wide_kv_weight, preferred_element_type=jnp.float32).astype(
        jnp.bfloat16
    )
    narrow_rows = jnp.dot(pieces[0], narrow_kv_weight, preferred_element_type=jnp.float32).astype(
        jnp.bfloat16
    )
    rot_rows = pieces[1]
    key_pos = jnp.arange(rot_rows.shape[0], dtype=jnp.int32)
    final_state = (
        update(initial[0], wide_q, WIDE_NOPE, wide_rows, rot_rows, positions, key_pos),
        update(initial[1], narrow_q, NARROW_NOPE, narrow_rows, rot_rows, positions, key_pos),
    )
    wide_state, narrow_state = final_state
    wide_att = (wide_state[2] / wide_state[1][..., None]).astype(jnp.bfloat16)
    narrow_att = (narrow_state[2] / narrow_state[1][..., None]).astype(jnp.bfloat16)
    partial_proj = jnp.einsum(
        "hqv,hvd->qd",
        wide_att,
        wide_out_weight.reshape(wide_count, WIDE_VALUE, D_MODEL),
        preferred_element_type=jnp.float32,
    )
    partial_proj = partial_proj + jnp.einsum(
        "hqv,hvd->qd",
        narrow_att,
        narrow_out_weight.reshape(narrow_count, NARROW_VALUE, D_MODEL),
        preferred_element_type=jnp.float32,
    )
    proj_sum = lax.psum(rounded(partial_proj).astype(jnp.bfloat16), "tp").astype(jnp.float32)
    stream = (residual.astype(jnp.float32) + rounded(proj_sum)).astype(jnp.bfloat16)
    normed = rms_scale(stream, norm_gain)
    shared_hidden = (
        jax.nn.silu(jnp.dot(normed, shared_gate, preferred_element_type=jnp.float32))
        * jnp.dot(normed, shared_up, preferred_element_type=jnp.float32)
    ).astype(jnp.bfloat16)
    shared_part = jnp.dot(shared_hidden, shared_down, preferred_element_type=jnp.float32)
    shared_out = rounded(
        lax.psum_scatter(
            rounded(shared_part).astype(jnp.bfloat16), "tp", scatter_dimension=1, tiled=True
        ).astype(jnp.float32)
    )
    top_count = route_ids.shape[1]
    local_experts = expert_gate.shape[0]
    sp_count = lax.axis_size("sp")
    expert_total = sp_count * local_experts
    capacity = max(2, 3 * tok_rows * top_count // (2 * expert_total))
    flat_ids = route_ids.reshape(-1)
    one_hot = (flat_ids[:, None] == jnp.arange(expert_total, dtype=jnp.int32)[None, :]).astype(
        jnp.int32
    )
    earlier = jnp.cumsum(one_hot, axis=0) - one_hot
    slot_index = flat_ids * capacity + jnp.sum(earlier * one_hot, axis=1)
    copy_token = jnp.arange(tok_rows * top_count, dtype=jnp.int32) // top_count
    source_row = jnp.zeros((expert_total * capacity,), jnp.int32).at[slot_index].set(copy_token)
    filled = jnp.zeros((expert_total * capacity,), jnp.bfloat16).at[slot_index].set(1.0)
    column_width = D_MODEL // lax.axis_size("tp")
    column_start = lax.axis_index("tp") * column_width
    own_normed = lax.dynamic_slice_in_dim(normed, column_start, column_width, 1)
    outgoing = (own_normed[source_row] * filled[:, None]).reshape(
        sp_count, local_experts, capacity, column_width
    )
    arrived = lax.all_gather(
        lax.all_to_all(outgoing, "sp", split_axis=0, concat_axis=0, tiled=True),
        "tp",
        axis=3,
        tiled=True,
    )
    gate_value = jnp.einsum(
        "sejd,edf->sejf", arrived, expert_gate, preferred_element_type=jnp.float32
    )
    up_value = jnp.einsum("sejd,edf->sejf", arrived, expert_up, preferred_element_type=jnp.float32)
    hidden_units = (jax.nn.silu(gate_value) * up_value).astype(jnp.bfloat16)
    down_part = jnp.einsum(
        "sejf,efd->sejd", hidden_units, expert_down, preferred_element_type=jnp.float32
    )
    expert_result = lax.psum_scatter(
        rounded(down_part).astype(jnp.bfloat16), "tp", scatter_dimension=3, tiled=True
    )
    returned = lax.all_to_all(expert_result, "sp", split_axis=0, concat_axis=0, tiled=True)
    back_rows = returned.reshape(expert_total * capacity, column_width)[slot_index]
    routed = jnp.sum(
        back_rows.astype(jnp.float32).reshape(tok_rows, top_count, column_width)
        * route_weights[:, :, None],
        axis=1,
    )
    own_stream = lax.dynamic_slice_in_dim(stream, column_start, column_width, 1).astype(jnp.float32)
    return (own_stream + shared_out + routed).astype(jnp.bfloat16)


def solution(mesh):
    placed = (
        P("sp", "tp"),
        P("sp", "tp"),
        P("sp", None),
        P("sp", None),
        P(),
        P(None, "tp"),
        P(None, "tp"),
        P("tp", None),
        P("tp", None),
        P("sp", None),
        P(),
        P("sp", None),
        P("sp", None),
        P("sp", None, "tp"),
        P("sp", None, "tp"),
        P("sp", "tp", None),
        P(None, "tp"),
        P(None, "tp"),
        P("tp", None),
    )
    return jax.shard_map(
        local, mesh=mesh, in_specs=placed, out_specs=P("sp", "tp"), check_vma=False
    )
```

profile of v0, /device:TPU:0, one launch (start us, length us, event | category | flops | bytes accessed | tf_op | source)
XLA Modules:
  0.0 202.1 jit_solution(8818083878113061387)
XLA Ops:
  6.6 1.2 reshape.171
  8.7 15.7 %all-gather = bf16[8,64,32]{1,2,0:T(8,128)(2,1)S(1)} all-gather(bf16[1,64,32]{1,2,0:T(8,128)(2,1)S(1)} %maximum_bitcast_fusion), channel_id=1, replica_groups=mesh['sp'=8,'tp'=4] {'sp'}, dimensions={0}, use_global_device_ids=true | all-gather | bytes 36864 | tf_op jit(solution)/shard_map/all_gather | solution.py:117
  24.5 1.0 fusion.63
  25.5 0.9 fusion.65
  26.4 14.7 %all_gather.9 = bf16[512,512]{1,0:T(8,128)(2,1)S(1)} all-gather(bf16[64,512]{1,0:T(8,128)(2,1)S(1)} %fusion.65), channel_id=1, replica_groups=mesh['sp'=8,'tp'=4] {'sp'}, dimensions={0}, use_global_device_ids=true | all-gather | bytes 589824 | tf_op jit(solution)/shard_map/all_gather | solution.py:116
  41.2 0.8 copy-done.1
  42.0 2.9 %convolution_convert_fusion.2 = bf16[512,1024]{1,0:T(8,128)(2,1)} fusion(bf16[512,512]{1,0:T(8,128)(2,1)S(1)} %all_gather.9, bf16[512,1024]{1,0:T(8,128)(2,1)} %param.24), kind=kOutput, calls=%fused_computation.16 | convolution fusion | flops 537395200 | bytes 2621440 | tf_op jit(solution)/shard_map/dot_general | solution.py:119
  44.9 1.9 reshape.172
  46.8 1.4 fusion.100
  48.2 1.3 copy.61
  50.5 1.7 convolution_convert_fusion.3
  52.7 0.8 copy-done.8
  53.7 2.8 %convolution_bitcast_fusion.1 = f32[64,2048]{1,0:T(8,128)} fusion(bf16[4,64,2048]{2,1,0:T(8,128)(2,1)} %bitcast.76, f32[4,64,512]{2,1,0:T(8,128)} %copy-done.8, bf16[512,4,128]{0,2,1:T(8,128)(2,1)S(1)} %bitcast.74, f32[4,64]{1,0:T(4,128)S(1)} %broadcast_maximum_fusion, pred[64,512]{1,0:T(8,128)(4,1)S(1)} %iota_compare_fusion, f32[4,64]{1,0:T(4,128)S(1)} %fusion.35), kind=kOutput, calls=%fused_computation.8 | convolution fusion | flops 84312064 | bytes 2396160 | tf_op jit(solution)/shard_map/hqv,hvd->qd/dot_general | solution.py:140
  56.5 2.6 %fusion.2 = bf16[64,2048]{1,0:T(8,128)(2,1)} fusion(f32[64,2048]{1,0:T(8,128)} %convolution_bitcast_fusion.1, bf16[4,128,2048]{2,1,0:T(8,128)(2,1)S(1)} %bitcast.72, bf16[512,4,128]{2,1,0:T(4,128)(2,1)S(1)} %copy-done.3, f32[4,64,512]{2,1,0:T(8,128)} %copy-done.7, f32[4,64]{1,0:T(4,128)S(1)} %broadcast_maximum_fusion.1, ...), kind=kOutput, calls=%fused_computation.9 | convolution fusion | flops 168493056 | bytes 3966976 | tf_op jit(solution)/shard_map/hqv,hvd->qd/dot_general | solution.py:134
  60.2 1.0 scatter_custom_fusion
  61.2 1.3 scatter_custom_fusion.1
  62.7 41.1 %all-reduce.2.cloned.1.call-done = bf16[64,2048]{1,0:T(8,128)(2,1)} async-done(((bf16[64,2048]{1,0:T(8,128)(2,1)}), bf16[64,2048]{1,0:T(8,128)(2,1)}) %all-reduce.2.cloned.1.call-update) | async-done | bytes 262160 | tf_op jit(solution)/shard_map/psum | solution.py:146
  103.8 1.1 fusion.28
  104.9 0.7 copy-done.5
  105.8 1.0 gather_fusion
  107.2 12.8 %all_to_all.10 = bf16[8,2,12,512]{3,1,2,0:T(2,128)(2,1)S(1)} all-to-all(bf16[8,2,12,512]{3,1,2,0:T(2,128)(2,1)S(1)} %copy.51), channel_id=1, replica_groups=mesh['sp'=8,'tp'=4] {'sp'}, dimensions={0} | all-to-all | bytes 393216 | tf_op jit(solution)/shard_map/all_to_all | solution.py:180
  120.1 13.1 %all_gather.11 = bf16[8,2,12,2048]{3,2,0,1:T(8,128)(2,1)S(1)} all-gather(bf16[8,2,12,512]{3,2,0,1:T(8,128)(2,1)S(1)} %copy.52), channel_id=1, replica_groups=mesh['sp'=8,'tp'=4] {'tp'}, dimensions={3}, use_global_device_ids=true | all-gather | bytes 983040 | tf_op jit(solution)/shard_map/all_gather | solution.py:179
  133.2 1.2 fusion.8
  134.4 4.2 %fusion = bf16[8,2,12,2048]{3,2,0,1:T(8,128)(2,1)} fusion(bf16[2,256,2048]{2,1,0:T(8,128)(2,1)} %param.34, bf16[8,2,12,2048]{3,2,0,1:T(8,128)(2,1)S(1)} %all_gather.11, bf16[2,2048,256]{2,1,0:T(8,128)(2,1)} %param.33, f32[8,2,12,256]{3,2,0,1:T(8,128)} %fusion.8), kind=kOutput, calls=%fused_computation.5 | convolution fusion | flops 403341312 | bytes 5963776 | tf_op jit(solution)/shard_map/sejf,efd->sejd/dot_general | solution.py:190
  138.6 1.6 fusion.101
  140.2 2.7 %convolution_convert_fusion.1 = bf16[64,2048]{1,0:T(8,128)(2,1)} fusion(bf16[256,2048]{1,0:T(8,128)(2,1)S(1)} %copy-done.6, bf16[64,2048]{1,0:T(8,128)(2,1)S(1)} %fusion.30, bf16[2048,256]{1,0:T(8,128)(2,1)} %param.36, f32[64,256]{1,0:T(8,128)S(1)} %fusion.101), kind=kOutput, calls=%fused_computation.10 | convolution fusion | flops 134447104 | bytes 2686976 | tf_op jit(solution)/shard_map/dot_general | solution.py:153
  143.0 22.4 %reduce-scatter.5.cloned.1.call-done = bf16[8,2,12,512]{3,2,0,1:T(8,128)(2,1)} async-done(((bf16[8,2,12,2048]{3,2,0,1:T(8,128)(2,1)}), bf16[8,2,12,512]{3,2,0,1:T(8,128)(2,1)}) %reduce-scatter.5.cloned.1.call-update) | async-done | bytes 196624 | tf_op jit(solution)/shard_map/reduce_scatter | solution.py:193
  165.4 1.8 copy.53
  167.2 4.6 %all-to-all-start.1 = ((bf16[8,2,12,512]{3,1,2,0:T(2,128)(2,1)}), bf16[8,2,12,512]{3,1,2,0:T(2,128)(2,1)S(1)}, u32[]{:S(2)}, u32[]{:S(2)}) async-start(bf16[8,2,12,512]{3,1,2,0:T(2,128)(2,1)} %copy.53), calls=%async_computation.3 | async-start | bytes 393216 | tf_op jit(solution)/shard_map/all_to_all | solution.py:196
  171.9 20.6 %reduce-scatter.3.cloned.1.call-done = bf16[64,512]{1,0:T(8,128)(2,1)} async-done(((bf16[64,2048]{1,0:T(8,128)(2,1)}), bf16[64,512]{1,0:T(8,128)(2,1)}) %reduce-scatter.3.cloned.1.call-update) | async-done | bytes 65552 | tf_op jit(solution)/shard_map/reduce_scatter | solution.py:155
  192.6 0.8 gather_fusion.1
  194.1 1.5 add_convert_fusion.1
  (92 shorter events, 5.2 us)
Async XLA Ops:
  6.5 50.0 %copy-start = (bf16[512,2048]{1,0:T(8,128)(2,1)S(1)}, bf16[512,2048]{1,0:T(8,128)(2,1)}, u32[]{:S(2)}) copy-start(bf16[512,2048]{1,0:T(8,128)(2,1)} %param.26) | copy-start | bytes 6291460
  6.5 97.2 %all-reduce.2.cloned.1.call-start = ((), (), s32[]{:S(2)}) async-start(), calls=%async_computation.4 | async-start | bytes 524288 | tf_op jit(solution)/shard_map/psum | solution.py:146
  7.7 37.2 %copy-start.9 = (bf16[64,4,160]{2,1,0:T(4,128)(2,1)}, bf16[64,4,160]{2,1,0:T(4,128)(2,1)S(1)}, u32[]{:S(2)}) copy-start(bf16[64,4,160]{2,1,0:T(4,128)(2,1)S(1)} %reshape.171) | copy-start | bytes 245764
  41.2 0.8 copy-start.1
  46.8 2.7 %copy-start.12 = (bf16[64,384]{1,0:T(8,128)(2,1)S(1)}, bf16[64,384]{1,0:T(8,128)(2,1)}, u32[]{:S(2)}) copy-start(bf16[64,384]{1,0:T(8,128)(2,1)} %param.20) | copy-start | bytes 147460
  46.8 3.1 %slice-start.1 = ((bf16[64,4,160]{2,1,0:T(4,128)(2,1)}), bf16[64,4,128]{2,1,0:T(4,128)(2,1)S(1)}, s32[]{:S(2)}) async-start(bf16[64,4,160]{2,1,0:T(4,128)(2,1)} %copy-done.9), calls=%async_computation.8 | async-start | bytes 131072 | tf_op jit(solution)/shard_map/slice | solution.py:103
  46.8 3.1 %slice-start = ((bf16[64,4,160]{2,1,0:T(4,128)(2,1)}), bf16[64,4,32]{2,1,0:T(4,128)(2,1)S(1)}, s32[]{:S(2)}) async-start(bf16[64,4,160]{2,1,0:T(4,128)(2,1)} %copy-done.9), calls=%async_computation.7 | async-start | bytes 131072 | tf_op jit(solution)/shard_map/slice | solution.py:103
  49.5 1.0 copy-start.2
  50.5 2.2 %copy-start.7 = (f32[4,64,512]{2,1,0:T(8,128)}, f32[4,64,512]{2,1,0:T(8,128)S(1)}, u32[]{:S(2)}) copy-start(f32[4,64,512]{2,1,0:T(8,128)S(1)} %get-tuple-element.24) | copy-start | bytes 1572868
  52.3 4.2 %copy-start.3 = (bf16[512,4,128]{2,1,0:T(4,128)(2,1)S(1)}, bf16[512,4,128]{2,1,0:T(4,128)(2,1)}, u32[]{:S(2)}) copy-start(bf16[512,4,128]{2,1,0:T(4,128)(2,1)} %get-tuple-element.9) | copy-start | bytes 1572868
  52.7 0.8 copy-start.8
  56.5 2.7 %copy-start.14 = (s32[64,2]{0,1:T(2,128)S(1)}, s32[64,2]{0,1:T(2,128)}, u32[]{:S(2)}) copy-start(s32[64,2]{0,1:T(2,128)} %param.30) | copy-start | bytes 1540
  56.5 47.2 %copy-start.10 = (bf16[64,2048]{1,0:T(8,128)(2,1)S(1)}, bf16[64,2048]{1,0:T(8,128)(2,1)}, u32[]{:S(2)}) copy-start(bf16[64,2048]{1,0:T(8,128)(2,1)} %param.28) | copy-start | bytes 786436
  56.5 49.1 %copy-start.13 = (f32[2048]{0:T(1024)S(1)}, f32[2048]{0:T(1024)}, u32[]{:S(2)}) copy-start(f32[2048]{0:T(1024)} %param.29) | copy-start | bytes 24580
  59.2 106.2 %reduce-scatter.5.cloned.1.call-start = ((), (), s32[]{:S(2)}) async-start(), calls=%async_computation.6 | async-start | bytes 1310720 | tf_op jit(solution)/shard_map/reduce_scatter | solution.py:193
  104.9 0.7 copy-start.5
  106.9 26.3 %copy-start.4 = (bf16[2,2048,256]{2,1,0:T(8,128)(2,1)S(1)}, bf16[2,2048,256]{2,1,0:T(8,128)(2,1)}, u32[]{:S(2)}) copy-start(bf16[2,2048,256]{2,1,0:T(8,128)(2,1)} %param.32) | copy-start | bytes 6291460
  138.5 1.7 copy-start.6
  138.5 54.0 %reduce-scatter.3.cloned.1.call-start = ((), (), s32[]{:S(2)}) async-start(), calls=%async_computation.5 | async-start | bytes 327680 | tf_op jit(solution)/shard_map/reduce_scatter | solution.py:155
  140.2 31.6 %copy-start.15 = (f32[64,2]{0,1:T(2,128)S(1)}, f32[64,2]{0,1:T(2,128)}, u32[]{:S(2)}) copy-start(f32[64,2]{0,1:T(2,128)} %param.31) | copy-start | bytes 1540
  167.2 25.3 %all-to-all-start.1 = ((bf16[8,2,12,512]{3,1,2,0:T(2,128)(2,1)}), bf16[8,2,12,512]{3,1,2,0:T(2,128)(2,1)S(1)}, u32[]{:S(2)}, u32[]{:S(2)}) async-start(bf16[8,2,12,512]{3,1,2,0:T(2,128)(2,1)} %copy.53), calls=%async_computation.3 | async-start | bytes 393216 | tf_op jit(solution)/shard_map/all_to_all | solution.py:196
  192.5 1.5 copy-start.11
Sparse Core Ops, SparseCore 0:
  59.3 44.4 all-reduce.1
  138.7 26.6 reduce-scatter.4
  168.1 24.3 reduce-scatter.2
where the time goes:
time: 203 us; the launch traced here: 202 us
  waiting for transfers between devices  84.1 us (41%)
  blocking collectives  56.4 us (28%)
  matrix products  20.4 us (10%)
  local copies, waits for them, and re-layouts  15.8 us (8%)
  between operations  13.6 us (7%)
  other arithmetic  6.96 us (3%)
  starting transfers between devices  4.71 us (2%)
    psum x1, waiting for transfers between devices, local(): lax.psum(rounded(partial_proj).astype(jnp.bfloat16), 'tp')  41.1 us
    reduce_scatter x1, waiting for transfers between devices, local(): lax.psum_scatter(rounded(down_part).astype(jnp.bfloat16), 'tp', scatter_d...  22.4 us
    reduce_scatter x1, waiting for transfers between devices, local(): lax.psum_scatter(rounded(shared_part).astype(jnp.bfloat16), 'tp', scatter...  20.6 us
    all_gather x1, blocking collectives, local(): lax.all_gather(key_rot, 'sp', axis=0, tiled=True)  15.7 us
    all_gather x1, blocking collectives, local(): lax.all_gather(latent, 'sp', axis=0, tiled=True)  14.7 us
    all_gather x1, blocking collectives, local(): lax.all_gather(lax.all_to_all(outgoing, 'sp', split_axis=0, concat_axis=0...  13.1 us
    all_to_all x1, blocking collectives, local(): lax.all_to_all(outgoing, 'sp', split_axis=0, concat_axis=0, tiled=True)  12.8 us
    all_to_all x1, starting transfers between devices, local(): lax.all_to_all(expert_result, 'sp', split_axis=0, concat_axis=0, tiled=True)  4.62 us
  transfers between devices with their start and end apart: 4, of which 3 were waited for; matrix products, arithmetic and copies ran while one was open for 5% of the time, Pallas kernels for 0%

commit v1 on v0

--- a/solution.py
+++ b/solution.py
@@ -143,7 +143,9 @@
         narrow_out_weight.reshape(narrow_count, NARROW_VALUE, D_MODEL),
         preferred_element_type=jnp.float32,
     )
-    proj_sum = lax.psum(rounded(partial_proj).astype(jnp.bfloat16), "tp").astype(jnp.float32)
+    proj_sum = jnp.sum(
+        lax.all_gather(rounded(partial_proj).astype(jnp.bfloat16), "tp"), axis=0
+    ).astype(jnp.float32)
     stream = (residual.astype(jnp.float32) + rounded(proj_sum)).astype(jnp.bfloat16)
     normed = rms_scale(stream, norm_gain)
     shared_hidden = (

time: 203 us -> 187 us (0.921)
  waiting for transfers between devices: 84.1 us -> 67.6 us
    psum x1 -> x0, waiting for transfers between devices: 41.1 us -> none  [local(): lax.psum(rounded(partial_proj).astype(jnp.bfloat16), 'tp')]
    all_gather x0 -> x1, waiting for transfers between devices: none -> 24.5 us  [local(): lax.all_gather(rounded(partial_proj).astype(jnp.bfloat16), 'tp')]
where the time goes in v1:
time: 187 us; the launch traced here: 186 us
  waiting for transfers between devices  67.6 us (36%)
  blocking collectives  56.4 us (30%)
  matrix products  20.5 us (11%)
  local copies, waits for them, and re-layouts  15.8 us (8%)
  between operations  13.6 us (7%)
  other arithmetic  7.42 us (4%)
  starting transfers between devices  4.68 us (3%)
    all_gather x1, waiting for transfers between devices, local(): lax.all_gather(rounded(partial_proj).astype(jnp.bfloat16), 'tp')  24.5 us
    reduce_scatter x1, waiting for transfers between devices, local(): lax.psum_scatter(rounded(down_part).astype(jnp.bfloat16), 'tp', scatter_d...  22.4 us
    reduce_scatter x1, waiting for transfers between devices, local(): lax.psum_scatter(rounded(shared_part).astype(jnp.bfloat16), 'tp', scatter...  20.6 us
    all_gather x1, blocking collectives, local(): lax.all_gather(key_rot, 'sp', axis=0, tiled=True)  15.7 us
    all_gather x1, blocking collectives, local(): lax.all_gather(latent, 'sp', axis=0, tiled=True)  14.7 us
    all_gather x1, blocking collectives, local(): lax.all_gather(lax.all_to_all(outgoing, 'sp', split_axis=0, concat_axis=0...  13.1 us
    all_to_all x1, blocking collectives, local(): lax.all_to_all(outgoing, 'sp', split_axis=0, concat_axis=0, tiled=True)  12.8 us
    all_to_all x1, starting transfers between devices, local(): lax.all_to_all(expert_result, 'sp', split_axis=0, concat_axis=0, tiled=True)  4.59 us
  transfers between devices with their start and end apart: 4, of which 3 were waited for; matrix products, arithmetic and copies ran while one was open for 5% of the time, Pallas kernels for 0%

profile of v1, /device:TPU:0, one launch (start us, length us, event | category | flops | bytes accessed | tf_op | source)
XLA Modules:
  0.0 186.0 jit_solution(11267310028610634815)
XLA Ops:
  6.6 1.2 reshape.171
  8.7 15.7 %all-gather.1 = bf16[8,64,32]{1,2,0:T(8,128)(2,1)S(1)} all-gather(bf16[1,64,32]{1,2,0:T(8,128)(2,1)S(1)} %maximum_bitcast_fusion), channel_id=1, replica_groups=mesh['sp'=8,'tp'=4] {'sp'}, dimensions={0}, use_global_device_ids=true | all-gather | bytes 36864 | tf_op jit(solution)/shard_map/all_gather | solution.py:117
  24.5 1.0 fusion.63
  25.5 0.9 fusion.65
  26.4 14.7 %all_gather.15 = bf16[512,512]{1,0:T(8,128)(2,1)S(1)} all-gather(bf16[64,512]{1,0:T(8,128)(2,1)S(1)} %fusion.65), channel_id=1, replica_groups=mesh['sp'=8,'tp'=4] {'sp'}, dimensions={0}, use_global_device_ids=true | all-gather | bytes 589824 | tf_op jit(solution)/shard_map/all_gather | solution.py:116
  41.2 0.8 copy-done.1
  42.0 2.9 %convolution_convert_fusion.2 = bf16[512,1024]{1,0:T(8,128)(2,1)} fusion(bf16[512,512]{1,0:T(8,128)(2,1)S(1)} %all_gather.15, bf16[512,1024]{1,0:T(8,128)(2,1)} %param.24), kind=kOutput, calls=%fused_computation.16 | convolution fusion | flops 537395200 | bytes 2621440 | tf_op jit(solution)/shard_map/dot_general | solution.py:119
  44.9 1.9 reshape.172
  46.8 1.4 fusion.100
  48.2 1.3 copy.61
  50.5 1.7 convolution_convert_fusion.3
  52.7 0.8 copy-done.8
  53.7 2.8 %convolution_bitcast_fusion.1 = f32[64,2048]{1,0:T(8,128)} fusion(bf16[4,64,2048]{2,1,0:T(8,128)(2,1)} %bitcast.78, f32[4,64,512]{2,1,0:T(8,128)} %copy-done.8, bf16[512,4,128]{0,2,1:T(8,128)(2,1)S(1)} %bitcast.75, f32[4,64]{1,0:T(4,128)S(1)} %broadcast_maximum_fusion, pred[64,512]{1,0:T(8,128)(4,1)S(1)} %iota_compare_fusion, f32[4,64]{1,0:T(4,128)S(1)} %fusion.35), kind=kOutput, calls=%fused_computation.8 | convolution fusion | flops 84312064 | bytes 2396160 | tf_op jit(solution)/shard_map/hqv,hvd->qd/dot_general | solution.py:140
  56.5 2.6 %fusion.2 = bf16[64,2048]{1,0:T(8,128)(2,1)} fusion(f32[64,2048]{1,0:T(8,128)} %convolution_bitcast_fusion.1, bf16[4,128,2048]{2,1,0:T(8,128)(2,1)S(1)} %bitcast.73, bf16[512,4,128]{2,1,0:T(4,128)(2,1)S(1)} %copy-done.3, f32[4,64,512]{2,1,0:T(8,128)} %copy-done.7, f32[4,64]{1,0:T(4,128)S(1)} %broadcast_maximum_fusion.1, ...), kind=kOutput, calls=%fused_computation.9 | convolution fusion | flops 168493056 | bytes 3966976 | tf_op jit(solution)/shard_map/hqv,hvd->qd/dot_general | solution.py:134
  60.2 1.0 scatter_custom_fusion
  61.2 1.3 scatter_custom_fusion.1
  62.7 24.5 %all-gather.4.cloned.1.call-done = bf16[256,2048]{1,0:T(8,128)(2,1)} async-done(((bf16[64,2048]{1,0:T(8,128)(2,1)}), bf16[256,2048]{1,0:T(8,128)(2,1)}) %all-gather.4.cloned.1.call-update) | async-done | bytes 1048592 | tf_op jit(solution)/shard_map/all_gather | solution.py:147
  87.2 1.4 reduce_sum.71
  88.8 0.7 copy-done.5
  89.7 1.0 gather_fusion
  91.1 12.8 %all_to_all.10 = bf16[8,2,12,512]{3,1,2,0:T(2,128)(2,1)S(1)} all-to-all(bf16[8,2,12,512]{3,1,2,0:T(2,128)(2,1)S(1)} %copy.51), channel_id=1, replica_groups=mesh['sp'=8,'tp'=4] {'sp'}, dimensions={0} | all-to-all | bytes 393216 | tf_op jit(solution)/shard_map/all_to_all | solution.py:182
  104.0 13.1 %all_gather.19 = bf16[8,2,12,2048]{3,2,0,1:T(8,128)(2,1)S(1)} all-gather(bf16[8,2,12,512]{3,2,0,1:T(8,128)(2,1)S(1)} %copy.52), channel_id=1, replica_groups=mesh['sp'=8,'tp'=4] {'tp'}, dimensions={3}, use_global_device_ids=true | all-gather | bytes 983040 | tf_op jit(solution)/shard_map/all_gather | solution.py:181
  117.1 1.2 fusion.8
  118.3 4.2 %fusion = bf16[8,2,12,2048]{3,2,0,1:T(8,128)(2,1)} fusion(bf16[2,256,2048]{2,1,0:T(8,128)(2,1)} %param.34, bf16[8,2,12,2048]{3,2,0,1:T(8,128)(2,1)S(1)} %all_gather.19, bf16[2,2048,256]{2,1,0:T(8,128)(2,1)} %param.33, f32[8,2,12,256]{3,2,0,1:T(8,128)} %fusion.8), kind=kOutput, calls=%fused_computation.5 | convolution fusion | flops 403341312 | bytes 5963776 | tf_op jit(solution)/shard_map/sejf,efd->sejd/dot_general | solution.py:192
  122.5 1.6 fusion.101
  124.1 2.7 %convolution_convert_fusion.1 = bf16[64,2048]{1,0:T(8,128)(2,1)} fusion(bf16[256,2048]{1,0:T(8,128)(2,1)S(1)} %copy-done.6, bf16[64,2048]{1,0:T(8,128)(2,1)S(1)} %fusion.30, bf16[2048,256]{1,0:T(8,128)(2,1)} %param.36, f32[64,256]{1,0:T(8,128)S(1)} %fusion.101), kind=kOutput, calls=%fused_computation.10 | convolution fusion | flops 134447104 | bytes 2686976 | tf_op jit(solution)/shard_map/dot_general | solution.py:155
  126.9 22.4 %reduce-scatter.5.cloned.1.call-done = bf16[8,2,12,512]{3,2,0,1:T(8,128)(2,1)} async-done(((bf16[8,2,12,2048]{3,2,0,1:T(8,128)(2,1)}), bf16[8,2,12,512]{3,2,0,1:T(8,128)(2,1)}) %reduce-scatter.5.cloned.1.call-update) | async-done | bytes 196624 | tf_op jit(solution)/shard_map/reduce_scatter | solution.py:195
  149.3 1.8 copy.53
  151.1 4.6 %all-to-all-start.1 = ((bf16[8,2,12,512]{3,1,2,0:T(2,128)(2,1)}), bf16[8,2,12,512]{3,1,2,0:T(2,128)(2,1)S(1)}, u32[]{:S(2)}, u32[]{:S(2)}) async-start(bf16[8,2,12,512]{3,1,2,0:T(2,128)(2,1)} %copy.53), calls=%async_computation.3 | async-start | bytes 393216 | tf_op jit(solution)/shard_map/all_to_all | solution.py:198
  155.8 20.6 %reduce-scatter.3.cloned.1.call-done = bf16[64,512]{1,0:T(8,128)(2,1)} async-done(((bf16[64,2048]{1,0:T(8,128)(2,1)}), bf16[64,512]{1,0:T(8,128)(2,1)}) %reduce-scatter.3.cloned.1.call-update) | async-done | bytes 65552 | tf_op jit(solution)/shard_map/reduce_scatter | solution.py:157
  176.5 0.8 gather_fusion.1
  178.0 1.5 add_convert_fusion.1
  (93 shorter events, 5.4 us)
Async XLA Ops:
  6.5 50.0 %copy-start = (bf16[512,2048]{1,0:T(8,128)(2,1)S(1)}, bf16[512,2048]{1,0:T(8,128)(2,1)}, u32[]{:S(2)}) copy-start(bf16[512,2048]{1,0:T(8,128)(2,1)} %param.26) | copy-start | bytes 6291460
  6.5 80.7 %all-gather.4.cloned.1.call-start = ((), (), s32[]{:S(2)}) async-start(), calls=%async_computation.6 | async-start | bytes 1310720 | tf_op jit(solution)/shard_map/all_gather | solution.py:147
  7.7 37.2 %copy-start.9 = (bf16[64,4,160]{2,1,0:T(4,128)(2,1)}, bf16[64,4,160]{2,1,0:T(4,128)(2,1)S(1)}, u32[]{:S(2)}) copy-start(bf16[64,4,160]{2,1,0:T(4,128)(2,1)S(1)} %reshape.171) | copy-start | bytes 245764
  41.2 0.8 copy-start.1
  46.8 2.7 %copy-start.12 = (bf16[64,384]{1,0:T(8,128)(2,1)S(1)}, bf16[64,384]{1,0:T(8,128)(2,1)}, u32[]{:S(2)}) copy-start(bf16[64,384]{1,0:T(8,128)(2,1)} %param.20) | copy-start | bytes 147460
  46.8 3.1 %slice-start.1 = ((bf16[64,4,160]{2,1,0:T(4,128)(2,1)}), bf16[64,4,128]{2,1,0:T(4,128)(2,1)S(1)}, s32[]{:S(2)}) async-start(bf16[64,4,160]{2,1,0:T(4,128)(2,1)} %copy-done.9), calls=%async_computation.8 | async-start | bytes 131072 | tf_op jit(solution)/shard_map/slice | solution.py:103
  46.8 3.1 %slice-start = ((bf16[64,4,160]{2,1,0:T(4,128)(2,1)}), bf16[64,4,32]{2,1,0:T(4,128)(2,1)S(1)}, s32[]{:S(2)}) async-start(bf16[64,4,160]{2,1,0:T(4,128)(2,1)} %copy-done.9), calls=%async_computation.7 | async-start | bytes 131072 | tf_op jit(solution)/shard_map/slice | solution.py:103
  49.5 1.0 copy-start.2
  50.5 2.2 %copy-start.7 = (f32[4,64,512]{2,1,0:T(8,128)}, f32[4,64,512]{2,1,0:T(8,128)S(1)}, u32[]{:S(2)}) copy-start(f32[4,64,512]{2,1,0:T(8,128)S(1)} %get-tuple-element.24) | copy-start | bytes 1572868
  52.3 4.2 %copy-start.3 = (bf16[512,4,128]{2,1,0:T(4,128)(2,1)S(1)}, bf16[512,4,128]{2,1,0:T(4,128)(2,1)}, u32[]{:S(2)}) copy-start(bf16[512,4,128]{2,1,0:T(4,128)(2,1)} %get-tuple-element.9) | copy-start | bytes 1572868
  52.7 0.8 copy-start.8
  56.5 2.7 %copy-start.14 = (s32[64,2]{0,1:T(2,128)S(1)}, s32[64,2]{0,1:T(2,128)}, u32[]{:S(2)}) copy-start(s32[64,2]{0,1:T(2,128)} %param.30) | copy-start | bytes 1540
  56.5 32.1 %copy-start.10 = (bf16[64,2048]{1,0:T(8,128)(2,1)S(1)}, bf16[64,2048]{1,0:T(8,128)(2,1)}, u32[]{:S(2)}) copy-start(bf16[64,2048]{1,0:T(8,128)(2,1)} %param.28) | copy-start | bytes 786436
  59.2 30.4 %copy-start.13 = (f32[2048]{0:T(1024)S(1)}, f32[2048]{0:T(1024)}, u32[]{:S(2)}) copy-start(f32[2048]{0:T(1024)} %param.29) | copy-start | bytes 24580
  59.2 90.1 %reduce-scatter.5.cloned.1.call-start = ((), (), s32[]{:S(2)}) async-start(), calls=%async_computation.5 | async-start | bytes 1310720 | tf_op jit(solution)/shard_map/reduce_scatter | solution.py:195
  88.8 0.7 copy-start.5
  90.8 26.3 %copy-start.4 = (bf16[2,2048,256]{2,1,0:T(8,128)(2,1)S(1)}, bf16[2,2048,256]{2,1,0:T(8,128)(2,1)}, u32[]{:S(2)}) copy-start(bf16[2,2048,256]{2,1,0:T(8,128)(2,1)} %param.32) | copy-start | bytes 6291460
  122.4 1.7 copy-start.6
  122.4 54.0 %reduce-scatter.3.cloned.1.call-start = ((), (), s32[]{:S(2)}) async-start(), calls=%async_computation.4 | async-start | bytes 327680 | tf_op jit(solution)/shard_map/reduce_scatter | solution.py:157
  124.1 31.6 %copy-start.15 = (f32[64,2]{0,1:T(2,128)S(1)}, f32[64,2]{0,1:T(2,128)}, u32[]{:S(2)}) copy-start(f32[64,2]{0,1:T(2,128)} %param.31) | copy-start | bytes 1540
  151.1 25.3 %all-to-all-start.1 = ((bf16[8,2,12,512]{3,1,2,0:T(2,128)(2,1)}), bf16[8,2,12,512]{3,1,2,0:T(2,128)(2,1)S(1)}, u32[]{:S(2)}, u32[]{:S(2)}) async-start(bf16[8,2,12,512]{3,1,2,0:T(2,128)(2,1)} %copy.53), calls=%async_computation.3 | async-start | bytes 393216 | tf_op jit(solution)/shard_map/all_to_all | solution.py:198
  176.4 1.5 copy-start.11
Sparse Core Ops, SparseCore 0:
  59.3 27.8 all-gather.3
  122.6 26.6 reduce-scatter.4
  152.1 24.3 reduce-scatter.2
